TPU v7x, 32 devices: a whole 2x2x4 slice. The times are simulated.
32 devices in a mesh: sp: 4 (over z), fs: 4 (over y, x), tp: 2 (over core).
Axes of the slice: x: 2, y: 2, z: 4, core: 2. Of those that a mesh axis runs over, the one named last changes fastest.
Arguments:
- activations: bfloat16 [4, 1024, 2048], P('fs', 'sp'), may hold values from -600 to 600
- norm_gain: float32 [2048], replicated, may hold values from 0.1 to 1.9
- w_conv_gate: bfloat16 [2048, 1024], P('sp', ('fs', 'tp')), may hold values from -0.125 to 0.125
- w_conv_mult: bfloat16 [2048, 1024], P('sp', ('fs', 'tp')), may hold values from -0.125 to 0.125
- w_conv_in: bfloat16 [2048, 1024], P('sp', ('fs', 'tp')), may hold values from -0.125 to 0.125
- conv_taps: float32 [3, 1024], replicated, may hold values from -3.5 to 3.5
- w_query: bfloat16 [2048, 1024], P('sp', ('fs', 'tp')), may hold values from -0.125 to 0.125
- w_key: bfloat16 [2048, 1024], P('sp', ('fs', 'tp')), may hold values from -0.125 to 0.125
- w_value: bfloat16 [2048, 1024], P('sp', ('fs', 'tp')), may hold values from -0.125 to 0.125
- w_input_gate: bfloat16 [2048, 8], replicated, may hold values from -0.125 to 0.125
- w_forget_gate: bfloat16 [2048, 8], replicated, may hold values from -0.125 to 0.125
- gate_bias: float32 [2, 8], replicated, may hold values from -1 to 120
- decay_shift: float32 [4, 1024, 8], P(None, 'sp'), may hold values from -2 to 0, as said below
- head_gain: float32 [1024], replicated, may hold values from 0.1 to 1.9
- w_out_conv: bfloat16 [1024, 2048], P(('fs', 'tp'), 'sp'), may hold values from -0.125 to 0.125
- w_out_mem: bfloat16 [1024, 2048], P(('fs', 'tp'), 'sp'), may hold values from -0.125 to 0.125
Outputs:
- output: bfloat16 [4, 1024, 2048], P('fs', ('sp', 'tp'))
Inputs may be any that keep to these rules, and one draw needn't show every extreme that they name: `decay_shift`: never positive.
All inputs are finite; a program needn't handle non-finite values.
Results may differ from a plain program's by a relative error of at most 0.015.
Values may be sent and summed in bfloat16 or wider, within the bound.
A program may use at most 64 MiB of HBM per device.

v0:
```python
import jax
import jax.numpy as jnp
from jax import lax
from jax.sharding import PartitionSpec as P

MEMORY_HEADS = 8
HEAD_DIM = 128
BLOCK = 64
EPSILON = 1e-06
FAR_BELOW = -1e30
HIGHEST_PRECISION = lax.Precision.HIGHEST


def prefix(value, axis, join, neutral):
    count, mine = (lax.axis_size(axis), lax.axis_index(axis))
    pieces = jax.tree.map(lambda part: lax.all_gather(part, axis), value)
    subtotal = jax.tree.map(
        lambda part, zero: jnp.full_like(part, 0) + jnp.asarray(zero, part.dtype), value, neutral
    )

    def lap(position, subtotal):
        longer = join(subtotal, jax.tree.map(lambda part: part[position], pieces))
        return jax.tree.map(lambda new, old: jnp.where(position < mine, new, old), longer, subtotal)

    return lax.fori_loop(0, count - 1, lap, subtotal)


def from_behind(array, axis, by):
    peers = lax.axis_size(axis)
    pairs = [(i, i + by) for i in range(peers) if 0 <= i + by < peers]
    return lax.ppermute(array, axis, pairs)


def combine_states(earlier, later):
    total_one, peak_one, state_one = earlier
    total_two, peak_two, state_two = later
    peak_new = jnp.maximum(total_two + peak_one, peak_two)
    scale_old = jnp.exp(total_two + peak_one - peak_new)
    scale_new = jnp.exp(peak_two - peak_new)
    return (
        total_one + total_two,
        peak_new,
        scale_old[..., None, None] * state_one + scale_new[..., None, None] * state_two,
    )


def head_rows(values, seq_count, heads_here):
    tokens = values.shape[1]
    split_heads = values.reshape(seq_count, tokens, heads_here, HEAD_DIM).transpose(0, 2, 1, 3)
    return split_heads.reshape(seq_count * heads_here, tokens, HEAD_DIM).astype(jnp.float32)


def gate_rows(values, seq_count, heads_here):
    tokens = values.shape[1]
    return values.transpose(0, 2, 1).reshape(seq_count * heads_here, tokens)


def memory_cell(query_rows, key_rows, value_rows, entry_gate, log_forget):
    members = query_rows.shape[0]
    tokens = query_rows.shape[1]
    head_width = query_rows.shape[2]
    nblocks = tokens // BLOCK
    block_shape = (members, nblocks, BLOCK, head_width)
    query_blocks = query_rows.reshape(block_shape)
    key_blocks = key_rows.reshape(block_shape) * head_width ** (-0.5)
    value_blocks = value_rows.reshape(block_shape)
    entry_blocks = entry_gate.reshape(members, nblocks, BLOCK)
    forget_sums = jnp.cumsum(log_forget.reshape(members, nblocks, BLOCK), axis=-1)
    block_total = forget_sums[..., -1]
    local_logs = block_total[..., None] - forget_sums + entry_blocks
    local_peak = jnp.max(local_logs, axis=-1)
    local_weights = jnp.exp(local_logs - local_peak[..., None])
    local_state = jnp.einsum(
        "bclv,bclk->bcvk",
        local_weights[..., None] * value_blocks,
        key_blocks,
        precision=HIGHEST_PRECISION,
    )

    def advance(running, block_item):
        return (combine_states(running, block_item), running)

    zero_sums = jnp.zeros((members,), jnp.float32)
    low_peaks = jnp.full((members,), FAR_BELOW, jnp.float32)
    zero_states = jnp.zeros((members, head_width, head_width), jnp.float32)
    block_items = (
        jnp.moveaxis(block_total, 1, 0),
        jnp.moveaxis(local_peak, 1, 0),
        jnp.moveaxis(local_state, 1, 0),
    )
    device_total, inner_states = lax.scan(advance, (zero_sums, low_peaks, zero_states), block_items)
    inner_states = tuple((jnp.moveaxis(tensor, 0, 1) for tensor in inner_states))
    total_sum, total_peak, total_state = device_total
    before = prefix(
        (total_sum, total_peak, total_state),
        "sp",
        combine_states,
        (zero_sums, low_peaks, zero_states),
    )
    opening = combine_states((zero_sums, zero_sums, zero_states), before)
    opening = tuple((tensor[:, None] for tensor in opening))
    _, prior_peak, prior_state = combine_states(opening, inner_states)
    positions = jnp.arange(BLOCK)
    causal_mask = positions[:, None] >= positions[None, :]
    pair_logs = jnp.where(
        causal_mask,
        forget_sums[..., :, None] - forget_sums[..., None, :] + entry_blocks[..., None, :],
        -jnp.inf,
    )
    carried_logs = forget_sums + prior_peak[..., None]
    row_peak = jnp.maximum(carried_logs, jnp.max(pair_logs, axis=-1))
    inner_weights = jnp.exp(pair_logs - row_peak[..., None])
    carried_weights = jnp.exp(carried_logs - row_peak)
    scores = inner_weights * jnp.einsum(
        "bcld,bcsd->bcls", query_blocks, key_blocks, precision=HIGHEST_PRECISION
    )
    numerator = carried_weights[..., None] * jnp.einsum(
        "bcvk,bclk->bclv", prior_state, query_blocks, precision=HIGHEST_PRECISION
    ) + jnp.einsum("bcls,bcsv->bclv", scores, value_blocks, precision=HIGHEST_PRECISION)
    return numerator.reshape(members, tokens, head_width)


def shards(
    activations,
    norm_gain,
    w_conv_gate,
    w_conv_mult,
    w_conv_in,
    conv_taps,
    w_query,
    w_key,
    w_value,
    w_input_gate,
    w_forget_gate,
    gate_bias,
    decay_shift,
    head_gain,
    w_out_conv,
    w_out_mem,
):
    group_index = lax.axis_index(("fs", "tp"))
    heads_here = MEMORY_HEADS // (lax.axis_size("fs") * lax.axis_size("tp"))
    channels = w_conv_gate.shape[1]
    sequences = lax.all_gather(activations, "fs", axis=0, tiled=True)
    seq_count = sequences.shape[0]
    tokens = sequences.shape[1]
    model_width = sequences.shape[2]
    row_count = seq_count * tokens
    flat_rows = sequences.reshape(row_count, model_width).astype(jnp.float32)
    normed = (
        flat_rows
        * lax.rsqrt(jnp.mean(flat_rows * flat_rows, axis=-1, keepdims=True) + EPSILON)
        * norm_gain
    ).astype(jnp.bfloat16)
    pieces = (
        lax.all_gather(w_conv_gate, "sp", axis=0, tiled=True),
        lax.all_gather(w_conv_mult, "sp", axis=0, tiled=True),
        lax.all_gather(w_conv_in, "sp", axis=0, tiled=True),
        lax.all_gather(w_query, "sp", axis=0, tiled=True),
        lax.all_gather(w_key, "sp", axis=0, tiled=True),
        lax.all_gather(w_value, "sp", axis=0, tiled=True),
    )
    projected = tuple(
        (jnp.dot(normed, shard_piece, preferred_element_type=jnp.float32) for shard_piece in pieces)
    )
    conv_gate, conv_mult, conv_in, query, keys_proj, value = [
        tensor.astype(jnp.bfloat16).reshape(seq_count, tokens, -1) for tensor in projected
    ]
    product = (conv_mult.astype(jnp.float32) * conv_in.astype(jnp.float32)).astype(jnp.bfloat16)
    ntaps = conv_taps.shape[0]
    rim_rows = from_behind(product[:, tokens - (ntaps - 1) :, :], "sp", 1)
    padded = jnp.concatenate([rim_rows, product], axis=1).astype(jnp.float32)
    tap_weights = lax.dynamic_slice_in_dim(conv_taps, group_index * channels, channels, 1)
    mixed_sum = jnp.zeros((seq_count, tokens, channels), jnp.float32)
    for tap_index in range(ntaps):
        mixed_sum = (
            mixed_sum + tap_weights[tap_index] * padded[:, tap_index : tap_index + tokens, :]
        )
    conv_out = (conv_gate.astype(jnp.float32) * mixed_sum).astype(jnp.bfloat16)
    entry_cols = lax.dynamic_slice_in_dim(w_input_gate, group_index * heads_here, heads_here, 1)
    forget_cols = lax.dynamic_slice_in_dim(w_forget_gate, group_index * heads_here, heads_here, 1)
    gate_values = jnp.dot(
        normed,
        jnp.concatenate([entry_cols, forget_cols], axis=1),
        preferred_element_type=jnp.float32,
    ).reshape(seq_count, tokens, 2 * heads_here)
    bias_rows = lax.dynamic_slice_in_dim(gate_bias, group_index * heads_here, heads_here, 1)
    decay_rows = lax.dynamic_slice_in_dim(decay_shift, group_index * heads_here, heads_here, 2)
    entry = gate_values[..., :heads_here] + bias_rows[0]
    log_forget = jax.nn.log_sigmoid(gate_values[..., heads_here:] + bias_rows[1]) + decay_rows
    cell = memory_cell(
        head_rows(query, seq_count, heads_here),
        head_rows(keys_proj, seq_count, heads_here),
        head_rows(value, seq_count, heads_here),
        gate_rows(entry, seq_count, heads_here),
        gate_rows(log_forget, seq_count, heads_here),
    )
    cell = cell * lax.rsqrt(jnp.mean(cell * cell, axis=-1, keepdims=True) + EPSILON)
    gain_rows = lax.dynamic_slice_in_dim(
        head_gain, group_index * heads_here * HEAD_DIM, heads_here * HEAD_DIM, 0
    ).reshape(1, heads_here, 1, HEAD_DIM)
    scaled = cell.reshape(seq_count, heads_here, tokens, HEAD_DIM) * gain_rows
    mem_out = (
        scaled.transpose(0, 2, 1, 3)
        .reshape(seq_count, tokens, heads_here * HEAD_DIM)
        .astype(jnp.bfloat16)
    )
    conv_seq, mem_seq = (
        lax.all_to_all(conv_out, "fs", split_axis=0, concat_axis=2, tiled=True),
        lax.all_to_all(mem_out, "fs", split_axis=0, concat_axis=2, tiled=True),
    )
    rows_conv, rows_mem = (
        lax.all_gather(w_out_conv, "fs", axis=0, tiled=True),
        lax.all_gather(w_out_mem, "fs", axis=0, tiled=True),
    )
    full_conv, full_mem = (
        lax.all_gather(rows_conv, "sp", axis=1, tiled=True),
        lax.all_gather(rows_mem, "sp", axis=1, tiled=True),
    )
    conv_flat = conv_seq[0]
    mem_flat = mem_seq[0]
    output = lax.psum_scatter(
        (
            jnp.dot(conv_flat, full_conv, preferred_element_type=jnp.float32)
            + jnp.dot(mem_flat, full_mem, preferred_element_type=jnp.float32)
        ).astype(jnp.bfloat16),
        "tp",
        scatter_dimension=0,
        tiled=True,
    ).astype(jnp.float32)
    return output.astype(jnp.bfloat16).reshape(1, output.shape[0], -1)


def solution(mesh):
    return jax.shard_map(
        shards,
        mesh=mesh,
        in_specs=(
            P("fs", "sp", None),
            P(),
            P("sp", ("fs", "tp")),
            P("sp", ("fs", "tp")),
            P("sp", ("fs", "tp")),
            P(),
            P("sp", ("fs", "tp")),
            P("sp", ("fs", "tp")),
            P("sp", ("fs", "tp")),
            P(),
            P(),
            P(),
            P(None, "sp", None),
            P(),
            P(("fs", "tp"), "sp"),
            P(("fs", "tp"), "sp"),
        ),
        out_specs=P("fs", ("sp", "tp"), None),
        check_vma=False,
    )
```

profile of v0, /device:TPU:0, one launch (start us, length us, event | category | flops | bytes accessed | tf_op | source)
XLA Modules:
  0.0 249.8 jit_solution(10992935933422332303)
XLA Ops:
  8.7 17.6 %all_gather.58 = bf16[2048,128]{1,0:T(8,128)(2,1)S(1)} all-gather(bf16[512,128]{1,0:T(8,128)(2,1)} %param.27), channel_id=1, replica_groups=mesh['sp'=4,'fs'=4,'tp'=2] {'sp'}, dimensions={0}, use_global_device_ids=true | all-gather | bytes 655360 | tf_op jit(solution)/shard_map/all_gather | solution.py:160
  26.3 16.6 %all_gather.57 = bf16[2048,128]{1,0:T(8,128)(2,1)S(1)} all-gather(bf16[512,128]{1,0:T(8,128)(2,1)} %param.28), channel_id=1, replica_groups=mesh['sp'=4,'fs'=4,'tp'=2] {'sp'}, dimensions={0}, use_global_device_ids=true | all-gather | bytes 655360 | tf_op jit(solution)/shard_map/all_gather | solution.py:161
  43.7 20.8 %all-gather.8.cloned.1.call-done = bf16[4,256,2048]{2,1,0:T(8,128)(2,1)} async-done(((bf16[1,256,2048]{2,1,0:T(8,128)(2,1)}), bf16[4,256,2048]{2,1,0:T(8,128)(2,1)}) %all-gather.8.cloned.1.call-update) | async-done | bytes 4194320 | tf_op jit(solution)/shard_map/all_gather | solution.py:144
  64.5 3.2 %multiply_reduce_fusion = f32[4,256]{1,0:T(4,128)S(1)} fusion(bf16[4,256,2048]{2,1,0:T(8,128)(2,1)} %all-gather.8.cloned.1.call-done), kind=kLoop, calls=%fused_computation.34 | loop fusion | flops 6290432 | bytes 4198400 | tf_op jit(solution)/shard_map/reduce_sum | solution.py:152
  69.2 2.2 fusion.43
  72.9 3.2 %fusion.14 = bf16[1024,2048]{1,0:T(8,128)(2,1)S(1)} fusion(bf16[4,256,2048]{2,1,0:T(8,128)(2,1)} %all-gather.8.cloned.1.call-done, f32[2048]{0:T(1024)S(1)} %copy-done.8, f32[1024]{0:T(1024)S(1)} %bitcast.163), kind=kLoop, calls=%fused_computation.32 | loop fusion | flops 8388608 | bytes 8400896 | tf_op jit(solution)/shard_map/convert_element_type | solution.py:154
  78.8 2.0 convolution_bitcast_fusion
  82.7 10.6 %all_gather.55 = bf16[512,512]{1,0:T(8,128)(2,1)} all-gather(bf16[128,512]{1,0:T(8,128)(2,1)S(1)} %copy-done.6), channel_id=1, replica_groups=mesh['sp'=4,'fs'=4,'tp'=2] {'fs'}, dimensions={0}, use_global_device_ids=true | all-gather | bytes 655360 | tf_op jit(solution)/shard_map/all_gather | solution.py:213
  93.4 10.4 %all_gather.66 = bf16[512,512]{1,0:T(8,128)(2,1)} all-gather(bf16[128,512]{1,0:T(8,128)(2,1)S(1)} %copy-done.7), channel_id=1, replica_groups=mesh['sp'=4,'fs'=4,'tp'=2] {'fs'}, dimensions={0}, use_global_device_ids=true | all-gather | bytes 655360 | tf_op jit(solution)/shard_map/all_gather | solution.py:214
  103.9 19.9 %all_gather.65 = bf16[2048,128]{1,0:T(8,128)(2,1)} all-gather(bf16[512,128]{1,0:T(8,128)(2,1)} %param.26), channel_id=1, replica_groups=mesh['sp'=4,'fs'=4,'tp'=2] {'sp'}, dimensions={0}, use_global_device_ids=true | all-gather | bytes 655360 | tf_op jit(solution)/shard_map/all_gather | solution.py:159
  123.8 20.8 %all_gather.53 = bf16[2048,128]{1,0:T(8,128)(2,1)S(1)} all-gather(bf16[512,128]{1,0:T(8,128)(2,1)} %param.23), channel_id=1, replica_groups=mesh['sp'=4,'fs'=4,'tp'=2] {'sp'}, dimensions={0}, use_global_device_ids=true | all-gather | bytes 655360 | tf_op jit(solution)/shard_map/all_gather | solution.py:157
  144.6 20.7 %all_gather.54 = bf16[2048,128]{1,0:T(8,128)(2,1)S(1)} all-gather(bf16[512,128]{1,0:T(8,128)(2,1)} %param.24), channel_id=1, replica_groups=mesh['sp'=4,'fs'=4,'tp'=2] {'sp'}, dimensions={0}, use_global_device_ids=true | all-gather | bytes 655360 | tf_op jit(solution)/shard_map/all_gather | solution.py:158
  166.3 20.4 %all_gather.52 = bf16[2048,128]{1,0:T(8,128)(2,1)} all-gather(bf16[512,128]{1,0:T(8,128)(2,1)} %param.22), channel_id=1, replica_groups=mesh['sp'=4,'fs'=4,'tp'=2] {'sp'}, dimensions={0}, use_global_device_ids=true | all-gather | bytes 655360 | tf_op jit(solution)/shard_map/all_gather | solution.py:156
  187.9 4.3 %convolution_convert_fusion = bf16[1024,128]{1,0:T(8,128)(2,1)} fusion(bf16[1024,2048]{1,0:T(8,128)(2,1)} %copy-done.1, bf16[2048,128]{1,0:T(8,128)(2,1)} %all_gather.65), kind=kOutput, calls=%fused_computation.45 | convolution fusion | flops 537001984 | bytes 4980736 | tf_op jit(solution)/shard_map/dot_general | solution.py:164
  195.0 2.1 collective-permute-start
  197.1 3.6 %convolution_convert_fusion.5 = bf16[1024,128]{1,0:T(8,128)(2,1)S(1)} fusion(bf16[1024,2048]{1,0:T(8,128)(2,1)} %copy-done.1, bf16[2048,128]{1,0:T(8,128)(2,1)} %all_gather.52), kind=kOutput, calls=%fused_computation.56 | convolution fusion | flops 537001984 | bytes 4980736 | tf_op jit(solution)/shard_map/dot_general | solution.py:164
  201.5 10.3 %all-reduce.2 = (f32[16]{0:T(128)S(1)}, f32[16]{0:T(128)S(1)}) all-reduce(f32[16]{0:T(128)S(1)} %dynamic-update-slice, f32[16]{0:T(128)S(1)} %dynamic-update-slice.1), channel_id=2, replica_groups=mesh['sp'=4,'fs'=4,'tp'=2] {'sp'}, use_global_device_ids=true, to_apply=%add | all-reduce | flops 32 | bytes 256
  213.5 3.4 %all-to-all-start = ((bf16[4,256,128]{1,2,0:T(8,128)(2,1)}), bf16[4,256,128]{1,2,0:T(8,128)(2,1)S(1)}, u32[]{:S(2)}, u32[]{:S(2)}) async-start(bf16[4,256,128]{1,2,0:T(8,128)(2,1)} %fusion.31), calls=%async_computation | async-start | bytes 524288 | tf_op jit(solution)/shard_map/all_to_all | solution.py:209
  216.9 3.4 %while.40 = (s32[]{:T(128)}, f32[4]{0:T(128)S(1)}, f32[4]{0:T(128)S(1)}, f32[4,128,128]{2,1,0:T(8,128)S(1)}, s32[]{:T(128)}, /*index=5*/f32[4,4]{1,0:T(4,128)S(1...) while((s32[]{:T(128)}, f32[4]{0:T(128)S(1)}, f32[4]{0:T(128)S(1)}, ...), condition=%wide.region_6.7_spmd.clone, body=%wide.region_5.6_spmd.clone.sunk | while | flops 327728 | bytes 786793 | solution.py:25
  224.1 4.1 %all-to-all-start.1 = ((bf16[4,256,128]{1,2,0:T(8,128)(2,1)}), bf16[4,256,128]{1,2,0:T(8,128)(2,1)S(1)}, u32[]{:S(2)}, u32[]{:S(2)}) async-start(bf16[4,256,128]{1,2,0:T(8,128)(2,1)} %multiply_convert_fusion.2), calls=%async_computation.1 | async-start | bytes 524288 | tf_op jit(solution)/shard_map/all_to_all | solution.py:210
  228.2 2.3 fusion.52
  230.5 3.0 %all-to-all-done.1 = bf16[4,256,128]{1,2,0:T(8,128)(2,1)S(1)} async-done(((bf16[4,256,128]{1,2,0:T(8,128)(2,1)}), bf16[4,256,128]{1,2,0:T(8,128)(2,1)S(1)}, u32[]{:S(2)}, u32[]{:S(2)}) %all-to-all-start.1) | async-done | bytes 262176 | tf_op jit(solution)/shard_map/all_to_all | solution.py:210
  233.5 3.3 %fusion.19 = bf16[256,2048]{1,0:T(8,128)(2,1)} fusion(f32[256,2048]{1,0:T(8,128)S(1)} %fusion.52, bf16[256,512]{0,1:T(8,128)(2,1)S(1)} %bitcast.159, bf16[512,2048]{1,0:T(8,128)(2,1)} %all-gather.12.cloned.1.call-done), kind=kOutput, calls=%fused_computation.40 | convolution fusion | flops 537919488 | bytes 5505024 | tf_op jit(solution)/shard_map/dot_general | solution.py:225
  236.9 6.4 %reduce-scatter.2.cloned.1.call-done = bf16[128,2048]{1,0:T(8,128)(2,1)} async-done(((bf16[256,2048]{1,0:T(8,128)(2,1)}), bf16[128,2048]{1,0:T(8,128)(2,1)}) %reduce-scatter.2.cloned.1.call-update) | async-done | bytes 524304 | tf_op jit(solution)/shard_map/reduce_scatter | solution.py:222
  (127 shorter events, 25.2 us)
Async XLA Ops:
  6.5 159.7 %copy-start = (f32[3,1024]{1,0:T(4,128)S(1)}, f32[3,1024]{1,0:T(4,128)}, u32[]{:S(2)}) copy-start(f32[3,1024]{1,0:T(4,128)} %param.25) | copy-start | bytes 36868
  6.5 61.2 %copy-start.8 = (f32[2048]{0:T(1024)S(1)}, f32[2048]{0:T(1024)}, u32[]{:S(2)}) copy-start(f32[2048]{0:T(1024)} %param.21) | copy-start | bytes 24580
  6.5 58.0 %all-gather.8.cloned.1.call-start = ((), (), s32[]{:S(2)}) async-start(), calls=%async_computation.3 | async-start | bytes 5242880 | tf_op jit(solution)/shard_map/all_gather | solution.py:144
  7.3 209.7 %all-gather.14.cloned.1.call-start = ((), (), s32[]{:S(2)}) async-start(), calls=%async_computation.7 | async-start | bytes 1310720 | tf_op jit(solution)/shard_map/all_gather | solution.py:16
  64.5 3.4 %copy-start.4 = (bf16[4,256,2048]{2,1,0:T(8,128)(2,1)S(1)}, bf16[4,256,2048]{2,1,0:T(8,128)(2,1)}, u32[]{:S(2)}) copy-start(bf16[4,256,2048]{2,1,0:T(8,128)(2,1)} %all-gather.8.cloned.1.call-done) | copy-start | bytes 12582916
  76.1 2.5 %copy-start.1 = (bf16[1024,2048]{1,0:T(8,128)(2,1)}, bf16[1024,2048]{1,0:T(8,128)(2,1)S(1)}, u32[]{:S(2)}) copy-start(bf16[1024,2048]{1,0:T(8,128)(2,1)S(1)} %fusion.14) | copy-start | bytes 12582916
  78.8 3.8 %copy-start.6 = (bf16[128,512]{1,0:T(8,128)(2,1)S(1)}, bf16[128,512]{1,0:T(8,128)(2,1)}, u32[]{:S(2)}) copy-start(bf16[128,512]{1,0:T(8,128)(2,1)} %param.34) | copy-start | bytes 393220
  80.8 12.6 %copy-start.7 = (bf16[128,512]{1,0:T(8,128)(2,1)S(1)}, bf16[128,512]{1,0:T(8,128)(2,1)}, u32[]{:S(2)}) copy-start(bf16[128,512]{1,0:T(8,128)(2,1)} %param.35) | copy-start | bytes 393220
  81.9 0.7 copy-start.3
  81.9 104.8 %copy-start.9 = (u32[32]{0:T(128)S(1)}, u32[32]{0:T(128)}, u32[]{:S(2)}) copy-start(u32[32]{0:T(128)} %constant.88) | copy-start | bytes 388
  82.6 145.5 %all-gather.10.cloned.1.call-start = ((), (), s32[]{:S(2)}) async-start(), calls=%async_computation.4 | async-start | bytes 2621440 | tf_op jit(solution)/shard_map/all_gather | solution.py:217
  93.3 137.2 %all-gather.12.cloned.1.call-start = ((), (), s32[]{:S(2)}) async-start(), calls=%async_computation.5 | async-start | bytes 2621440 | tf_op jit(solution)/shard_map/all_gather | solution.py:218
  165.3 26.9 %copy-start.2 = (bf16[1024,2048]{1,0:T(8,128)(2,1)S(1)}, bf16[1024,2048]{1,0:T(8,128)(2,1)}, u32[]{:S(2)}) copy-start(bf16[1024,2048]{1,0:T(8,128)(2,1)} %copy-done.1) | copy-start | bytes 12582916
  195.0 17.2 %collective-permute-start = (bf16[4,2,128]{1,2,0:T(8,128)(2,1)S(1)}, bf16[4,2,128]{1,2,0:T(8,128)(2,1)S(1)}, u32[]{:S(2)}, u32[]{:S(2)}) collective-permute-start(bf16[4,2,128]{1,2,0:T(8,128)(2,1)S(1)} %slice.48), channel_id=1, source_target_pairs={{0,8},{8,16},{16,24},{1,9},{9,17},{17,25},{2,10},{10,18},{18,26},{... | collective-permute-start | bytes 6152 | tf_op jit(solution)/shard_map/ppermute | solution.py:31
  212.2 8.5 %copy-start.5 = (bf16[1024,128]{1,0:T(8,128)(2,1)S(1)}, bf16[1024,128]{1,0:T(8,128)(2,1)}, u32[]{:S(2)}) copy-start(bf16[1024,128]{1,0:T(8,128)(2,1)} %convolution_convert_fusion) | copy-start | bytes 786436
  213.5 10.6 %all-to-all-start = ((bf16[4,256,128]{1,2,0:T(8,128)(2,1)}), bf16[4,256,128]{1,2,0:T(8,128)(2,1)S(1)}, u32[]{:S(2)}, u32[]{:S(2)}) async-start(bf16[4,256,128]{1,2,0:T(8,128)(2,1)} %fusion.31), calls=%async_computation | async-start | bytes 524288 | tf_op jit(solution)/shard_map/all_to_all | solution.py:209
  224.1 9.5 %all-to-all-start.1 = ((bf16[4,256,128]{1,2,0:T(8,128)(2,1)}), bf16[4,256,128]{1,2,0:T(8,128)(2,1)S(1)}, u32[]{:S(2)}, u32[]{:S(2)}) async-start(bf16[4,256,128]{1,2,0:T(8,128)(2,1)} %multiply_convert_fusion.2), calls=%async_computation.1 | async-start | bytes 524288 | tf_op jit(solution)/shard_map/all_to_all | solution.py:210
  228.2 15.1 %reduce-scatter.2.cloned.1.call-start = ((), (), s32[]{:S(2)}) async-start(), calls=%async_computation.6 | async-start | bytes 1572864 | tf_op jit(solution)/shard_map/reduce_scatter | solution.py:222
Sparse Core Ops, SparseCore 0:
  9.2 55.2 all-gather.7
  82.8 31.4 all-gather.13
  115.9 67.3 all-gather.9
  184.7 44.9 all-gather.11
  237.0 6.2 reduce-scatter.1
where the time goes:
time: 251 us; the launch traced here: 250 us
  blocking collectives  147 us (59%)
  waiting for transfers between devices  31.1 us (12%)
  matrix products  24 us (10%)
  other arithmetic  16.5 us (7%)
  between operations  14.2 us (6%)
  starting transfers between devices  9.73 us (4%)
  local copies, waits for them, and re-layouts  6.76 us (3%)
    all_gather x1, waiting for transfers between devices, shards(): sequences = lax.all_gather(activations, 'fs', axis=0, tiled=True)  20.8 us
    all_gather x1, blocking collectives, shards(): lax.all_gather(w_conv_mult, 'sp', axis=0, tiled=True)  20.8 us
    all_gather x1, blocking collectives, shards(): lax.all_gather(w_conv_in, 'sp', axis=0, tiled=True)  20.7 us
    all_gather x1, blocking collectives, shards(): lax.all_gather(w_conv_gate, 'sp', axis=0, tiled=True)  20.4 us
    all_gather x1, blocking collectives, shards(): lax.all_gather(w_query, 'sp', axis=0, tiled=True)  19.9 us
    all_gather x1, blocking collectives, shards(): lax.all_gather(w_key, 'sp', axis=0, tiled=True)  17.6 us
    all_gather x1, blocking collectives, shards(): lax.all_gather(w_value, 'sp', axis=0, tiled=True)  16.6 us
    dot_general x6, matrix products, shards(): jnp.dot(normed, shard_piece, preferred_element_type=jnp.float32)  12.9 us
  transfers between devices with their start and end apart: 8, of which 3 were waited for; matrix products, arithmetic and copies ran while one was open for 10% of the time, Pallas kernels for 0%

commit v1 on v0

--- a/solution.py
+++ b/solution.py
@@ -158,7 +158,9 @@
         lax.all_gather(w_conv_in, "sp", axis=0, tiled=True),
         lax.all_gather(w_query, "sp", axis=0, tiled=True),
         lax.all_gather(w_key, "sp", axis=0, tiled=True),
-        lax.all_gather(w_value, "sp", axis=0, tiled=True),
+        jnp.concatenate(
+            lax.all_to_all(jnp.stack([w_value] * lax.axis_size("sp")), "sp", 0, 0), axis=0
+        ),
     )
     projected = tuple(
         (jnp.dot(normed, shard_piece, preferred_element_type=jnp.float32) for shard_piece in pieces)

time: 251 us -> 260 us (1.036)
  blocking collectives: 147 us -> 136 us
  starting transfers between devices: 9.73 us -> 16 us
  matrix products: 24 us -> 28.3 us
  local copies, waits for them, and re-layouts: 6.76 us -> 10.5 us
  waiting for transfers between devices: 31.1 us -> 34.4 us
  other arithmetic: 16.5 us -> 19.4 us
    all_gather x1 -> x0, blocking collectives: 16.6 us -> none  [shards(): lax.all_gather(w_value, 'sp', axis=0, tiled=True)]
    all_to_all x0 -> x1, starting transfers between devices: none -> 6.35 us  [shards(): lax.all_to_all(jnp.stack([w_value] * lax.axis_size('sp')), 'sp', 0, 0)]
    all_gather x1, blocking collectives: 17.6 us -> 22.8 us  [shards(): lax.all_gather(w_key, 'sp', axis=0, tiled=True)]
    dot_general x6, matrix products: 12.9 us -> 17.2 us  [shards(): jnp.dot(normed, shard_piece, preferred_element_type=jnp.float32)]
    all_gather x1, waiting for transfers between devices: 20.8 us -> 24.1 us  [shards(): sequences = lax.all_gather(activations, 'fs', axis=0, tiled=True)]
    convert_element_type x1 -> x2, other arithmetic: 3.2 us -> 6.19 us  [shards(): normed = (flat_rows * lax.rsqrt(jnp.mean(flat_rows * flat_rows, axis=-1,...]
  transfers between devices with their start and end apart: 8 -> 9, of which waited for: 3 -> 3; matrix products, arithmetic and copies ran while one was open for 10% -> 18% of each run, Pallas kernels for 0% -> 0%
where the time goes in v1:
time: 260 us; the launch traced here: 259 us
  blocking collectives  136 us (52%)
  waiting for transfers between devices  34.4 us (13%)
  matrix products  28.3 us (11%)
  other arithmetic  19.4 us (7%)
  starting transfers between devices  16 us (6%)
  between operations  14.2 us (5%)
  local copies, waits for them, and re-layouts  10.5 us (4%)
    all_gather x1, waiting for transfers between devices, shards(): sequences = lax.all_gather(activations, 'fs', axis=0, tiled=True)  24.1 us
    all_gather x1, blocking collectives, shards(): lax.all_gather(w_key, 'sp', axis=0, tiled=True)  22.8 us
    all_gather x1, blocking collectives, shards(): lax.all_gather(w_conv_mult, 'sp', axis=0, tiled=True)  20.8 us
    all_gather x1, blocking collectives, shards(): lax.all_gather(w_conv_in, 'sp', axis=0, tiled=True)  20.7 us
    all_gather x1, blocking collectives, shards(): lax.all_gather(w_conv_gate, 'sp', axis=0, tiled=True)  20.5 us
    all_gather x1, blocking collectives, shards(): lax.all_gather(w_query, 'sp', axis=0, tiled=True)  19.9 us
    dot_general x6, matrix products, shards(): jnp.dot(normed, shard_piece, preferred_element_type=jnp.float32)  17.2 us
    all_gather x1, blocking collectives, shards(): lax.all_gather(w_out_conv, 'fs', axis=0, tiled=True)  10.6 us
  transfers between devices with their start and end apart: 9, of which 3 were waited for; matrix products, arithmetic and copies ran while one was open for 18% of the time, Pallas kernels for 0%

profile of v1, /device:TPU:0, one launch (start us, length us, event | category | flops | bytes accessed | tf_op | source)
XLA Modules:
  0.0 258.9 jit_solution(7497748061594863083)
XLA Ops:
  9.0 6.3 %all-to-all-start.1 = ((bf16[4,512,128]{2,1,0:T(8,128)(2,1)}), bf16[4,512,128]{2,1,0:T(8,128)(2,1)S(1)}, u32[]{:S(2)}, u32[]{:S(2)}) async-start(bf16[4,512,128]{2,1,0:T(8,128)(2,1)} %stack.2), calls=%async_computation.1 | async-start | bytes 1048576 | tf_op jit(solution)/shard_map/all_to_all | solution.py:162
  16.8 22.8 %all_gather.54 = bf16[2048,128]{1,0:T(8,128)(2,1)S(1)} all-gather(bf16[512,128]{1,0:T(8,128)(2,1)} %param.27), channel_id=1, replica_groups=mesh['sp'=4,'fs'=4,'tp'=2] {'sp'}, dimensions={0}, use_global_device_ids=true | all-gather | bytes 655360 | tf_op jit(solution)/shard_map/all_gather | solution.py:160
  40.4 24.1 %all-gather.8.cloned.1.call-done = bf16[4,256,2048]{2,1,0:T(8,128)(2,1)} async-done(((bf16[1,256,2048]{2,1,0:T(8,128)(2,1)}), bf16[4,256,2048]{2,1,0:T(8,128)(2,1)}) %all-gather.8.cloned.1.call-update) | async-done | bytes 4194320 | tf_op jit(solution)/shard_map/all_gather | solution.py:144
  64.5 3.2 %multiply_reduce_fusion = f32[4,256]{1,0:T(4,128)S(1)} fusion(bf16[4,256,2048]{2,1,0:T(8,128)(2,1)} %all-gather.8.cloned.1.call-done), kind=kLoop, calls=%fused_computation.34 | loop fusion | flops 6290432 | bytes 4198400 | tf_op jit(solution)/shard_map/reduce_sum | solution.py:152
  75.3 5.2 %fusion.14 = bf16[1024,2048]{1,0:T(8,128)(2,1)} fusion(bf16[4,256,2048]{2,1,0:T(8,128)(2,1)} %all-gather.8.cloned.1.call-done, f32[2048]{0:T(1024)S(1)} %copy-done.8, f32[1024]{0:T(1024)S(1)} %bitcast.168), kind=kLoop, calls=%fused_computation.32 | loop fusion | flops 8388608 | bytes 8400896 | tf_op jit(solution)/shard_map/convert_element_type | solution.py:154
  81.1 3.4 %fusion.18 = f32[1024,128]{1,0:T(8,128)S(1)} fusion(bf16[1024,2048]{1,0:T(8,128)(2,1)} %fusion.14, bf16[2048,128]{1,0:T(8,128)(2,1)S(1)} %all_gather.54), kind=kOutput, calls=%fused_computation.44 | convolution fusion | flops 537264128 | bytes 5242880 | tf_op jit(solution)/shard_map/dot_general | solution.py:166
  84.5 3.4 %convolution_convert_fusion.2 = bf16[1024,128]{1,0:T(8,128)(2,1)S(1)} fusion(bf16[1024,2048]{1,0:T(8,128)(2,1)} %bitcast.152, bf16[2048,128]{1,0:T(8,128)(2,1)S(1)} %bitcast.164), kind=kOutput, calls=%fused_computation.45 | convolution fusion | flops 537001984 | bytes 4980736 | tf_op jit(solution)/shard_map/dot_general | solution.py:166
  91.8 10.6 %all_gather.52 = bf16[512,512]{1,0:T(8,128)(2,1)} all-gather(bf16[128,512]{1,0:T(8,128)(2,1)S(1)} %copy-done.6), channel_id=1, replica_groups=mesh['sp'=4,'fs'=4,'tp'=2] {'fs'}, dimensions={0}, use_global_device_ids=true | all-gather | bytes 655360 | tf_op jit(solution)/shard_map/all_gather | solution.py:215
  102.5 10.5 %all_gather.62 = bf16[512,512]{1,0:T(8,128)(2,1)} all-gather(bf16[128,512]{1,0:T(8,128)(2,1)S(1)} %copy-done.7), channel_id=1, replica_groups=mesh['sp'=4,'fs'=4,'tp'=2] {'fs'}, dimensions={0}, use_global_device_ids=true | all-gather | bytes 655360 | tf_op jit(solution)/shard_map/all_gather | solution.py:216
  113.1 19.9 %all_gather.61 = bf16[2048,128]{1,0:T(8,128)(2,1)} all-gather(bf16[512,128]{1,0:T(8,128)(2,1)} %param.26), channel_id=1, replica_groups=mesh['sp'=4,'fs'=4,'tp'=2] {'sp'}, dimensions={0}, use_global_device_ids=true | all-gather | bytes 655360 | tf_op jit(solution)/shard_map/all_gather | solution.py:159
  133.0 20.8 %all_gather.50 = bf16[2048,128]{1,0:T(8,128)(2,1)S(1)} all-gather(bf16[512,128]{1,0:T(8,128)(2,1)} %param.23), channel_id=1, replica_groups=mesh['sp'=4,'fs'=4,'tp'=2] {'sp'}, dimensions={0}, use_global_device_ids=true | all-gather | bytes 655360 | tf_op jit(solution)/shard_map/all_gather | solution.py:157
  153.8 20.7 %all_gather.51 = bf16[2048,128]{1,0:T(8,128)(2,1)S(1)} all-gather(bf16[512,128]{1,0:T(8,128)(2,1)} %param.24), channel_id=1, replica_groups=mesh['sp'=4,'fs'=4,'tp'=2] {'sp'}, dimensions={0}, use_global_device_ids=true | all-gather | bytes 655360 | tf_op jit(solution)/shard_map/all_gather | solution.py:158
  175.4 20.5 %all_gather.49 = bf16[2048,128]{1,0:T(8,128)(2,1)} all-gather(bf16[512,128]{1,0:T(8,128)(2,1)} %param.22), channel_id=1, replica_groups=mesh['sp'=4,'fs'=4,'tp'=2] {'sp'}, dimensions={0}, use_global_device_ids=true | all-gather | bytes 655360 | tf_op jit(solution)/shard_map/all_gather | solution.py:156
  197.1 4.3 %convolution_convert_fusion = bf16[1024,128]{1,0:T(8,128)(2,1)} fusion(bf16[1024,2048]{1,0:T(8,128)(2,1)} %fusion.14, bf16[2048,128]{1,0:T(8,128)(2,1)} %all_gather.61), kind=kOutput, calls=%fused_computation.41 | convolution fusion | flops 537001984 | bytes 4980736 | tf_op jit(solution)/shard_map/dot_general | solution.py:166
  204.1 2.1 collective-permute-start
  206.2 3.6 %convolution_convert_fusion.5 = bf16[1024,128]{1,0:T(8,128)(2,1)S(1)} fusion(bf16[1024,2048]{1,0:T(8,128)(2,1)} %fusion.14, bf16[2048,128]{1,0:T(8,128)(2,1)} %all_gather.49), kind=kOutput, calls=%fused_computation.52 | convolution fusion | flops 537001984 | bytes 4980736 | tf_op jit(solution)/shard_map/dot_general | solution.py:166
  210.7 10.3 %all-reduce.2 = (f32[16]{0:T(128)S(1)}, f32[16]{0:T(128)S(1)}) all-reduce(f32[16]{0:T(128)S(1)} %dynamic-update-slice, f32[16]{0:T(128)S(1)} %dynamic-update-slice.1), channel_id=2, replica_groups=mesh['sp'=4,'fs'=4,'tp'=2] {'sp'}, use_global_device_ids=true, to_apply=%add | all-reduce | flops 32 | bytes 256
  222.6 3.4 %all-to-all-start = ((bf16[4,256,128]{1,2,0:T(8,128)(2,1)}), bf16[4,256,128]{1,2,0:T(8,128)(2,1)S(1)}, u32[]{:S(2)}, u32[]{:S(2)}) async-start(bf16[4,256,128]{1,2,0:T(8,128)(2,1)} %fusion.27), calls=%async_computation | async-start | bytes 524288 | tf_op jit(solution)/shard_map/all_to_all | solution.py:211
  226.0 3.4 %while.40 = (s32[]{:T(128)}, f32[4]{0:T(128)S(1)}, f32[4]{0:T(128)S(1)}, f32[4,128,128]{2,1,0:T(8,128)S(1)}, s32[]{:T(128)}, /*index=5*/f32[4,4]{1,0:T(4,128)S(1...) while((s32[]{:T(128)}, f32[4]{0:T(128)S(1)}, f32[4]{0:T(128)S(1)}, ...), condition=%wide.region_6.7_spmd.clone, body=%wide.region_5.6_spmd.clone.sunk | while | flops 327728 | bytes 786793 | solution.py:25
  233.2 4.1 %all-to-all-start.2 = ((bf16[4,256,128]{1,2,0:T(8,128)(2,1)}), bf16[4,256,128]{1,2,0:T(8,128)(2,1)S(1)}, u32[]{:S(2)}, u32[]{:S(2)}) async-start(bf16[4,256,128]{1,2,0:T(8,128)(2,1)} %multiply_convert_fusion.1), calls=%async_computation.2 | async-start | bytes 524288 | tf_op jit(solution)/shard_map/all_to_all | solution.py:212
  237.3 2.3 fusion.49
  239.6 3.0 %all-to-all-done.2 = bf16[4,256,128]{1,2,0:T(8,128)(2,1)S(1)} async-done(((bf16[4,256,128]{1,2,0:T(8,128)(2,1)}), bf16[4,256,128]{1,2,0:T(8,128)(2,1)S(1)}, u32[]{:S(2)}, u32[]{:S(2)}) %all-to-all-start.2) | async-done | bytes 262176 | tf_op jit(solution)/shard_map/all_to_all | solution.py:212
  242.6 3.3 %fusion.15 = bf16[256,2048]{1,0:T(8,128)(2,1)} fusion(f32[256,2048]{1,0:T(8,128)S(1)} %fusion.49, bf16[256,512]{0,1:T(8,128)(2,1)S(1)} %bitcast.163, bf16[512,2048]{1,0:T(8,128)(2,1)} %all-gather.12.cloned.1.call-done), kind=kOutput, calls=%fused_computation.36 | convolution fusion | flops 537919488 | bytes 5505024 | tf_op jit(solution)/shard_map/dot_general | solution.py:227
  246.0 6.4 %reduce-scatter.2.cloned.1.call-done = bf16[128,2048]{1,0:T(8,128)(2,1)} async-done(((bf16[256,2048]{1,0:T(8,128)(2,1)}), bf16[128,2048]{1,0:T(8,128)(2,1)}) %reduce-scatter.2.cloned.1.call-update) | async-done | bytes 524304 | tf_op jit(solution)/shard_map/reduce_scatter | solution.py:224
  (130 shorter events, 31.4 us)
Async XLA Ops:
  6.5 168.8 %copy-start = (f32[3,1024]{1,0:T(4,128)S(1)}, f32[3,1024]{1,0:T(4,128)}, u32[]{:S(2)}) copy-start(f32[3,1024]{1,0:T(4,128)} %param.25) | copy-start | bytes 36868
  6.5 61.2 %copy-start.8 = (f32[2048]{0:T(1024)S(1)}, f32[2048]{0:T(1024)}, u32[]{:S(2)}) copy-start(f32[2048]{0:T(1024)} %param.21) | copy-start | bytes 24580
  6.5 58.0 %all-gather.8.cloned.1.call-start = ((), (), s32[]{:S(2)}) async-start(), calls=%async_computation.4 | async-start | bytes 5242880 | tf_op jit(solution)/shard_map/all_gather | solution.py:144
  9.0 75.5 %all-to-all-start.1 = ((bf16[4,512,128]{2,1,0:T(8,128)(2,1)}), bf16[4,512,128]{2,1,0:T(8,128)(2,1)S(1)}, u32[]{:S(2)}, u32[]{:S(2)}) async-start(bf16[4,512,128]{2,1,0:T(8,128)(2,1)} %stack.2), calls=%async_computation.1 | async-start | bytes 1048576 | tf_op jit(solution)/shard_map/all_to_all | solution.py:162
  15.4 210.7 %all-gather.14.cloned.1.call-start = ((), (), s32[]{:S(2)}) async-start(), calls=%async_computation.8 | async-start | bytes 1310720 | tf_op jit(solution)/shard_map/all_gather | solution.py:16
  64.5 3.4 %copy-start.2 = (bf16[4,256,2048]{2,1,0:T(8,128)(2,1)S(1)}, bf16[4,256,2048]{2,1,0:T(8,128)(2,1)}, u32[]{:S(2)}) copy-start(bf16[4,256,2048]{2,1,0:T(8,128)(2,1)} %all-gather.8.cloned.1.call-done) | copy-start | bytes 12582916
  69.0 2.0 copy-start.4
  88.0 3.9 %copy-start.6 = (bf16[128,512]{1,0:T(8,128)(2,1)S(1)}, bf16[128,512]{1,0:T(8,128)(2,1)}, u32[]{:S(2)}) copy-start(bf16[128,512]{1,0:T(8,128)(2,1)} %param.34) | copy-start | bytes 393220
  90.0 12.6 %copy-start.7 = (bf16[128,512]{1,0:T(8,128)(2,1)S(1)}, bf16[128,512]{1,0:T(8,128)(2,1)}, u32[]{:S(2)}) copy-start(bf16[128,512]{1,0:T(8,128)(2,1)} %param.35) | copy-start | bytes 393220
  91.1 0.7 copy-start.3
  91.1 104.8 %copy-start.9 = (u32[32]{0:T(128)S(1)}, u32[32]{0:T(128)}, u32[]{:S(2)}) copy-start(u32[32]{0:T(128)} %constant.88) | copy-start | bytes 388
  91.8 145.5 %all-gather.10.cloned.1.call-start = ((), (), s32[]{:S(2)}) async-start(), calls=%async_computation.5 | async-start | bytes 2621440 | tf_op jit(solution)/shard_map/all_gather | solution.py:219
  102.5 137.1 %all-gather.12.cloned.1.call-start = ((), (), s32[]{:S(2)}) async-start(), calls=%async_computation.6 | async-start | bytes 2621440 | tf_op jit(solution)/shard_map/all_gather | solution.py:220
  174.4 26.9 %copy-start.1 = (bf16[1024,2048]{1,0:T(8,128)(2,1)S(1)}, bf16[1024,2048]{1,0:T(8,128)(2,1)}, u32[]{:S(2)}) copy-start(bf16[1024,2048]{1,0:T(8,128)(2,1)} %fusion.14) | copy-start | bytes 12582916
  204.1 17.2 %collective-permute-start = (bf16[4,2,128]{1,2,0:T(8,128)(2,1)S(1)}, bf16[4,2,128]{1,2,0:T(8,128)(2,1)S(1)}, u32[]{:S(2)}, u32[]{:S(2)}) collective-permute-start(bf16[4,2,128]{1,2,0:T(8,128)(2,1)S(1)} %slice.48), channel_id=1, source_target_pairs={{0,8},{8,16},{16,24},{1,9},{9,17},{17,25},{2,10},{10,18},{18,26},{... | collective-permute-start | bytes 6152 | tf_op jit(solution)/shard_map/ppermute | solution.py:31
  221.3 8.5 %copy-start.5 = (bf16[1024,128]{1,0:T(8,128)(2,1)S(1)}, bf16[1024,128]{1,0:T(8,128)(2,1)}, u32[]{:S(2)}) copy-start(bf16[1024,128]{1,0:T(8,128)(2,1)} %convolution_convert_fusion) | copy-start | bytes 786436
  222.6 10.6 %all-to-all-start = ((bf16[4,256,128]{1,2,0:T(8,128)(2,1)}), bf16[4,256,128]{1,2,0:T(8,128)(2,1)S(1)}, u32[]{:S(2)}, u32[]{:S(2)}) async-start(bf16[4,256,128]{1,2,0:T(8,128)(2,1)} %fusion.27), calls=%async_computation | async-start | bytes 524288 | tf_op jit(solution)/shard_map/all_to_all | solution.py:211
  233.2 9.5 %all-to-all-start.2 = ((bf16[4,256,128]{1,2,0:T(8,128)(2,1)}), bf16[4,256,128]{1,2,0:T(8,128)(2,1)S(1)}, u32[]{:S(2)}, u32[]{:S(2)}) async-start(bf16[4,256,128]{1,2,0:T(8,128)(2,1)} %multiply_convert_fusion.1), calls=%async_computation.2 | async-start | bytes 524288 | tf_op jit(solution)/shard_map/all_to_all | solution.py:212
  237.3 15.1 %reduce-scatter.2.cloned.1.call-start = ((), (), s32[]{:S(2)}) async-start(), calls=%async_computation.7 | async-start | bytes 1572864 | tf_op jit(solution)/shard_map/reduce_scatter | solution.py:224
Sparse Core Ops, SparseCore 0:
  9.2 55.2 all-gather.7
  91.9 31.4 all-gather.13
  125.0 67.3 all-gather.9
  193.9 44.9 all-gather.11
  246.1 6.2 reduce-scatter.1
